TPU v7x, 32 devices: a whole 2x2x4 slice. The times are simulated.
32 devices in a mesh: gr: 2 (over core), fs: 8 (over z, y), tp: 2 (over x).
Axes of the slice: x: 2, y: 2, z: 4, core: 2. Of those that a mesh axis runs over, the one named last changes fastest.
Arguments:
- tokens: bfloat16 [2048, 2048], P(('gr', 'fs')), may hold values from -60 to 60
- route_ids: int32 [2048, 2], P(('gr', 'fs')), may hold values from 0 to 7, all different within a row; in each aligned block of 128 rows (0 to 127, 128 to 255, ...) at most 32 rows name the same one
- route_logits: float32 [2048, 2], P(('gr', 'fs')), may hold values from -8 to 8
- norm_gain: float32 [2048], P(('gr', 'fs')), may hold values from 0.1 to 1.9
- gate_master: float32 [8, 2048, 7168], P(None, ('gr', 'fs'), 'tp'), may hold values from -0.125 to 0.125
- up_master: float32 [8, 2048, 7168], P(None, ('gr', 'fs'), 'tp'), may hold values from -0.125 to 0.125
- down_master: float32 [8, 7168, 2048], P(None, 'fs', ('gr', 'tp')), may hold values from -0.0625 to 0.0625
Outputs:
- gate_weight: bfloat16 [8, 2048, 7168], P('tp', None, 'fs')
- up_weight: bfloat16 [8, 2048, 7168], P('tp', None, 'fs')
- down_weight: bfloat16 [8, 7168, 2048], P('tp', 'fs')
- mixed: bfloat16 [2048, 2048], P(('gr', 'fs'))
Inputs may be any that keep to these rules, and one draw needn't show every extreme that they name: `route_ids`: in the rows of one device, that is in each aligned block of 128 rows, each of the 8 experts is named by exactly 32 rows; a row names two different experts.
All inputs are finite; a program needn't handle non-finite values.
Results may differ from a plain program's by a relative error of at most 0.025.
Values may be sent and summed in bfloat16 or wider, within the bound.
A program may use at most 192 MiB of HBM per device.

v0:
```python
import jax
import jax.numpy as jnp
from jax import lax
from jax.sharding import PartitionSpec as P

CAP = 32


epsilon = 1e-06


def local(tokens, route_ids, route_logits, norm_gain, gate_master, up_master, down_master):
    gain_rows = norm_gain[None, :, None]
    gate_half = (gate_master * gain_rows).astype(jnp.bfloat16)
    up_half = (up_master * gain_rows).astype(jnp.bfloat16)
    down_half = down_master.astype(jnp.bfloat16)
    gate_cols, up_cols, down_cols = (
        lax.all_to_all(gate_half, "tp", split_axis=0, concat_axis=2, tiled=True),
        lax.all_to_all(up_half, "tp", split_axis=0, concat_axis=2, tiled=True),
        lax.all_to_all(down_half, "tp", split_axis=0, concat_axis=2, tiled=True),
    )
    gate_part, up_part = (
        lax.all_to_all(gate_cols, "fs", split_axis=2, concat_axis=1, tiled=True),
        lax.all_to_all(up_cols, "fs", split_axis=2, concat_axis=1, tiled=True),
    )
    gate_weight, up_weight, down_weight = (
        lax.all_gather(gate_part, "gr", axis=1, tiled=True),
        lax.all_gather(up_part, "gr", axis=1, tiled=True),
        lax.all_gather(down_cols, "gr", axis=2, tiled=True),
    )
    as_float = tokens.astype(jnp.float32)
    normed = (
        as_float * lax.rsqrt(jnp.mean(as_float * as_float, axis=-1, keepdims=True) + epsilon)
    ).astype(jnp.bfloat16)
    differ = route_logits[:, 0] - route_logits[:, 1]
    route_weight = jnp.stack([jax.nn.sigmoid(differ), jax.nn.sigmoid(-differ)], axis=1)
    experts_here = gate_weight.shape[0]
    first_expert = lax.axis_index("tp") * experts_here
    expert_ids = first_expert + jnp.arange(experts_here, dtype=jnp.int32)
    route_hits = route_ids[None, :, :] == expert_ids[:, None, None]
    chosen = jnp.any(route_hits, axis=2)
    weight_rows = jnp.sum(jnp.where(route_hits, route_weight[None, :, :], 0.0), axis=2)
    slot_rank = jnp.cumsum(chosen.astype(jnp.int32), axis=1) - 1
    slot_ids = jnp.arange(CAP, dtype=jnp.int32)
    picker = chosen[:, None, :] & (slot_rank[:, None, :] == slot_ids[None, :, None])
    picker_float = picker.astype(jnp.float32)
    packed = jnp.einsum(
        "xsr,rd->sxd", picker.astype(jnp.bfloat16), normed, preferred_element_type=jnp.float32
    ).astype(jnp.bfloat16)
    slot_weight = jnp.einsum(
        "xsr,xr->sx", picker_float, weight_rows, precision=lax.Precision.HIGHEST
    )
    pieces = lax.all_gather(packed, "fs", axis=0, tiled=True)
    gate_act = jnp.einsum("kxd,xdh->kxh", pieces, gate_weight, preferred_element_type=jnp.float32)
    up_act = jnp.einsum("kxd,xdh->kxh", pieces, up_weight, preferred_element_type=jnp.float32)
    hidden = (jax.nn.silu(gate_act) * up_act).astype(jnp.bfloat16)
    expert_out = lax.psum_scatter(
        jnp.einsum("kxh,xhd->kxd", hidden, down_weight, preferred_element_type=jnp.float32).astype(
            jnp.bfloat16
        ),
        "fs",
        scatter_dimension=0,
        tiled=True,
    ).astype(jnp.float32)
    weighted = expert_out * slot_weight[:, :, None]
    block_sum = jnp.einsum("xsr,sxd->rd", picker_float, weighted, precision=lax.Precision.HIGHEST)
    mixed = lax.psum(block_sum.astype(jnp.bfloat16), "tp")
    return (gate_weight, up_weight, down_weight, mixed)


def solution(mesh):
    placed = (
        P(("gr", "fs"), None),
        P(("gr", "fs"), None),
        P(("gr", "fs"), None),
        P(("gr", "fs")),
        P(None, ("gr", "fs"), "tp"),
        P(None, ("gr", "fs"), "tp"),
        P(None, "fs", ("gr", "tp")),
    )
    return jax.shard_map(
        local,
        mesh=mesh,
        in_specs=placed,
        out_specs=(
            P("tp", None, "fs"),
            P("tp", None, "fs"),
            P("tp", "fs", None),
            P(("gr", "fs"), None),
        ),
        check_vma=False,
    )
```

profile of v0, /device:TPU:0, one launch (start us, length us, event | category | flops | bytes accessed | tf_op | source)
XLA Modules:
  0.0 955.7 jit_solution(9054798759361544984)
XLA Ops:
  7.2 13.3 %multiply_convert_fusion = (bf16[8,128,3584]{2,1,0:T(8,128)(2,1)S(1)}, bf16[8,128,3584]{2,1,0:T(8,128)(2,1)}) fusion(f32[8,128,3584]{2,1,0:T(8,128)} %param.12, f32[128]{0:T(128)} %param.10, f32[8,128,3584]{2,1,0:T(8,128)} %param.11), kind=kLoop, calls=%fused_computation | loop fusion | flops 14680064 | bytes 44040704 | tf_op jit(solution)/shard_map/convert_element_type | solution.py:15
  20.4 86.8 %all_to_all.90 = bf16[8,128,3584]{2,1,0:T(8,128)(2,1)} all-to-all(bf16[8,128,3584]{2,1,0:T(8,128)(2,1)S(1)} %get-tuple-element.26), channel_id=1, replica_groups=mesh['gr'=2,'fs'=8,'tp'=2] {'tp'}, dimensions={0} | all-to-all | bytes 14680064 | tf_op jit(solution)/shard_map/all_to_all | solution.py:19
  107.2 10.0 %copy.50 = bf16[4,128,2,3584]{1,3,2,0:T(8,128)(2,1)} copy(bf16[4,128,2,3584]{3,1,0,2:T(8,128)(2,1)} %bitcast.70) | data formatting | bytes 14680064 | tf_op jit(solution)/shard_map/all_to_all | solution.py:19
  117.2 10.9 %copy.51 = bf16[4,128,7168]{1,0,2:T(4,128)(2,1)} copy(bf16[4,128,7168]{1,2,0:T(8,128)(2,1)} %bitcast.71) | data formatting | bytes 14680064 | tf_op jit(solution)/shard_map/all_to_all | solution.py:19
  137.2 207.5 %all-to-all-done.3 = bf16[4,128,7168]{1,0,2:T(4,128)(2,1)} async-done(((bf16[4,128,7168]{1,0,2:T(4,128)(2,1)}), bf16[4,128,7168]{1,0,2:T(4,128)(2,1)}, u32[]{:S(2)}, u32[]{:S(2)}) %all-to-all-start.3) | async-done | bytes 7340064 | tf_op jit(solution)/shard_map/all_to_all | solution.py:24
  344.7 7.1 copy.52
  351.7 10.9 %copy.53 = bf16[4,8,128,896]{3,2,1,0:T(8,128)(2,1)} copy(bf16[4,8,128,896]{2,3,1,0:T(8,128)(2,1)} %bitcast.72) | data formatting | bytes 14680064 | tf_op jit(solution)/shard_map/all_to_all | solution.py:24
  362.6 11.0 %copy.54 = bf16[4,1024,896]{1,2,0:T(8,128)(2,1)} copy(bf16[4,1024,896]{2,1,0:T(8,128)(2,1)} %bitcast.73) | data formatting | bytes 14680064 | tf_op jit(solution)/shard_map/all_to_all | solution.py:24
  373.7 11.7 %convert_element_type.47 = bf16[8,896,512]{2,1,0:T(8,128)(2,1)} convert(f32[8,896,512]{2,1,0:T(8,128)} %param.13) | non-fusion elementwise | flops 3670016 | bytes 22020096 | tf_op jit(solution)/shard_map/convert_element_type | solution.py:16
  385.4 89.0 %all_to_all.91 = bf16[8,896,512]{2,1,0:T(8,128)(2,1)} all-to-all(bf16[8,896,512]{2,1,0:T(8,128)(2,1)} %convert_element_type.47), channel_id=1, replica_groups=mesh['gr'=2,'fs'=8,'tp'=2] {'tp'}, dimensions={0} | all-to-all | bytes 14680064 | tf_op jit(solution)/shard_map/all_to_all | solution.py:20
  481.0 14.7 %copy.66 = bf16[2,4,896,512]{3,0,2,1:T(2,128)(2,1)} copy(bf16[2,4,896,512]{3,2,1,0:T(8,128)(2,1)} %bitcast.69) | data formatting | bytes 14680064 | tf_op jit(solution)/shard_map/all_to_all | solution.py:20
  495.7 12.6 %all_to_all.84 = bf16[4,896,1024]{2,1,0:T(8,128)(2,1)} reshape(bf16[4,896,2,512]{3,2,1,0:T(2,128)(2,1)} %bitcast.74) | data formatting | bytes 14680064 | tf_op jit(solution)/shard_map/all_to_all | solution.py:20
  508.4 50.4 %all-to-all-done = bf16[8,128,3584]{2,1,0:T(8,128)(2,1)} async-done(((bf16[8,128,3584]{2,1,0:T(8,128)(2,1)}), bf16[8,128,3584]{2,1,0:T(8,128)(2,1)}, u32[]{:S(2)}, u32[]{:S(2)}) %all-to-all-start) | async-done | bytes 7340064 | tf_op jit(solution)/shard_map/all_to_all | solution.py:18
  558.8 10.0 %copy.46 = bf16[4,128,2,3584]{1,3,2,0:T(8,128)(2,1)} copy(bf16[4,128,2,3584]{3,1,0,2:T(8,128)(2,1)} %bitcast.1) | data formatting | bytes 14680064 | tf_op jit(solution)/shard_map/all_to_all | solution.py:18
  568.7 9.0 copy.47
  577.7 167.5 %all_to_all.92 = bf16[4,128,7168]{1,0,2:T(4,128)(2,1)S(1)} all-to-all(bf16[4,128,7168]{1,0,2:T(4,128)(2,1)S(1)} %copy.47), channel_id=1, replica_groups=mesh['gr'=2,'fs'=8,'tp'=2] {'fs'}, dimensions={2} | all-to-all | bytes 14680064 | tf_op jit(solution)/shard_map/all_to_all | solution.py:23
  749.2 8.2 copy.65
  757.6 14.5 %fusion.28 = f32[4,896,256]{2,1,0:T(8,128)} fusion(bf16[4,2048,896]{1,2,0:T(8,128)(2,1)} %all-gather.7.cloned.1.call-done, bf16[256,4,2048]{2,0,1:T(8,128)(2,1)} %all-gather.11.cloned.1.call-done), kind=kOutput, calls=%fused_computation.46 | convolution fusion | flops 3758096384 | bytes 22544384 | tf_op jit(solution)/shard_map/kxd,xdh->kxh/dot_general | solution.py:55
  772.1 10.6 %all-gather.5.cloned.1.call-done = bf16[4,2048,896]{1,2,0:T(8,128)(2,1)} async-done(((bf16[4,1024,896]{1,2,0:T(8,128)(2,1)}), bf16[4,2048,896]{1,2,0:T(8,128)(2,1)}) %all-gather.5.cloned.1.call-update) | async-done | bytes 14680080 | tf_op jit(solution)/shard_map/all_gather | solution.py:27
  782.7 17.6 %convert_bitcast_fusion = bf16[256,4,2048]{2,0,1:T(8,128)(2,1)} fusion(bf16[4,896,2048]{2,1,0:T(8,128)(2,1)} %all-gather.9.cloned.1.call-done, f32[4,896,256]{2,1,0:T(8,128)} %fusion.28, bf16[4,2048,896]{1,2,0:T(8,128)(2,1)} %all-gather.5.cloned.1.call-done, bf16[256,4,2048]{2,0,1:T(8,128)(2,1)} %all-gather.11.cloned.1.call-done), kind=kOutput, calls=%fused_computation.4 | convolution fusion | flops 7523794944 | bytes 41418752 | tf_op jit(solution)/shard_map/kxh,xhd->kxd/dot_general | solution.py:58
  800.7 89.6 %reduce-scatter.2.cloned.1.call-done = bf16[32,4,2048]{2,0,1:T(8,128)(2,1)} async-done(((bf16[256,4,2048]{2,0,1:T(8,128)(2,1)}), bf16[32,4,2048]{2,0,1:T(8,128)(2,1)}) %reduce-scatter.2.cloned.1.call-update) | async-done | bytes 524304 | tf_op jit(solution)/shard_map/reduce_scatter | solution.py:57
  893.0 20.7 %copy.58 = bf16[4,2048,896]{2,1,0:T(8,128)(2,1)} copy(bf16[4,2048,896]{1,2,0:T(8,128)(2,1)} %all-gather.7.cloned.1.call-done) | data formatting | bytes 29360128
  913.7 20.8 %copy.57 = bf16[4,2048,896]{2,1,0:T(8,128)(2,1)} copy(bf16[4,2048,896]{1,2,0:T(8,128)(2,1)} %all-gather.5.cloned.1.call-done) | data formatting | bytes 29360128
  934.5 13.5 %copy.69 = bf16[4,896,2048]{2,1,0:T(8,128)(2,1)} copy(bf16[4,896,2048]{2,1,0:T(8,128)(2,1)} %all-gather.9.cloned.1.call-done) | data formatting | bytes 29360128
  (55 shorter events, 23.7 us)
Async XLA Ops:
  128.1 6.2 copy-start.6
  128.1 7.1 copy-start
  128.1 216.6 %all-to-all-start.3 = ((bf16[4,128,7168]{1,0,2:T(4,128)(2,1)}), bf16[4,128,7168]{1,0,2:T(4,128)(2,1)}, u32[]{:S(2)}, u32[]{:S(2)}) async-start(bf16[4,128,7168]{1,0,2:T(4,128)(2,1)} %copy.51), calls=%async_computation.3 | async-start | bytes 14680064 | tf_op jit(solution)/shard_map/all_to_all | solution.py:24
  134.2 623.3 %all-gather.11.cloned.1.call-start = ((), (), s32[]{:S(2)}) async-start(), calls=%async_computation.9 | async-start | bytes 4718592 | tf_op jit(solution)/shard_map/all_gather | solution.py:53
  134.3 0.6 copy-start.8
  134.8 216.9 %copy-start.4 = (pred[4,128]{1,0:T(4,128)(4,1)}, pred[4,128]{1,0:T(4,128)(4,1)S(1)}, u32[]{:S(2)}) copy-start(pred[4,128]{1,0:T(4,128)(4,1)S(1)} %compare_reduce_fusion) | copy-start | bytes 1540
  135.4 0.5 copy-start.2
  137.1 620.5 %all-gather.7.cloned.1.call-start = ((), (), s32[]{:S(2)}) async-start(), calls=%async_computation.7 | async-start | bytes 22020096 | tf_op jit(solution)/shard_map/all_gather | solution.py:28
  474.4 84.4 %all-to-all-start = ((bf16[8,128,3584]{2,1,0:T(8,128)(2,1)}), bf16[8,128,3584]{2,1,0:T(8,128)(2,1)}, u32[]{:S(2)}, u32[]{:S(2)}) async-start(bf16[8,128,3584]{2,1,0:T(8,128)(2,1)} %get-tuple-element.27), calls=%async_computation | async-start | bytes 14680064 | tf_op jit(solution)/shard_map/all_to_all | solution.py:18
  481.0 291.1 %all-gather.9.cloned.1.call-start = ((), (), s32[]{:S(2)}) async-start(), calls=%async_computation.8 | async-start | bytes 22020096 | tf_op jit(solution)/shard_map/all_gather | solution.py:29
  508.3 274.4 %all-gather.5.cloned.1.call-start = ((), (), s32[]{:S(2)}) async-start(), calls=%async_computation.6 | async-start | bytes 22020096 | tf_op jit(solution)/shard_map/all_gather | solution.py:27
  757.5 132.9 %reduce-scatter.2.cloned.1.call-start = ((), (), s32[]{:S(2)}) async-start(), calls=%async_computation.10 | async-start | bytes 4718592 | tf_op jit(solution)/shard_map/reduce_scatter | solution.py:57
  772.1 28.3 %copy-start.10 = (f32[128,2]{0,1:T(2,128)S(1)}, f32[128,2]{0,1:T(2,128)}, u32[]{:S(2)}) copy-start(f32[128,2]{0,1:T(2,128)} %param.9) | copy-start | bytes 3076
  772.1 28.4 %copy-start.7 = (s32[128,2]{0,1:T(2,128)S(1)}, s32[128,2]{0,1:T(2,128)}, u32[]{:S(2)}) copy-start(s32[128,2]{0,1:T(2,128)} %param.8) | copy-start | bytes 3076
  772.1 28.4 %copy-start.9 = (s32[4]{0:T(128)S(1)}, s32[4]{0:T(128)}, u32[]{:S(2)}) copy-start(s32[4]{0:T(128)} %copy-done.8) | copy-start | bytes 52
  772.1 28.5 %copy-start.3 = (s32[4,128]{1,0:T(4,128)S(1)}, s32[4,128]{1,0:T(4,128)}, u32[]{:S(2)}) copy-start(s32[4,128]{1,0:T(4,128)} %copy-done.2) | copy-start | bytes 6148
  772.1 28.4 %copy-start.5 = (pred[4,128]{1,0:T(4,128)(4,1)S(1)}, pred[4,128]{1,0:T(4,128)(4,1)}, u32[]{:S(2)}) copy-start(pred[4,128]{1,0:T(4,128)(4,1)} %copy-done.4) | copy-start | bytes 1540
  800.3 134.2 %all-reduce.2.cloned.1.call-start = ((), (), s32[]{:S(2)}) async-start(), calls=%async_computation.11 | async-start | bytes 1048576 | tf_op jit(solution)/shard_map/psum | solution.py:67
  934.5 13.5 %copy-start.1 = (bf16[128,2048]{1,0:T(8,128)(2,1)S(1)}, bf16[128,2048]{1,0:T(8,128)(2,1)}, u32[]{:S(2)}) copy-start(bf16[128,2048]{1,0:T(8,128)(2,1)} %all-reduce.2.cloned.1.call-done) | copy-start | bytes 1572868
Sparse Core Ops, SparseCore 0:
  137.8 185.7 all-gather.10
  373.8 25.0 all-gather.6
  508.5 28.5 all-gather.8
  757.6 25.1 all-gather.4
  800.5 89.8 reduce-scatter.1
  893.1 28.2 all-reduce.1
where the time goes:
time: 959 us; the launch traced here: 956 us
  waiting for transfers between devices  358 us (37%)
  blocking collectives  343 us (36%)
  local copies, waits for them, and re-layouts  165 us (17%)
  matrix products  36.1 us (4%)
  other arithmetic  25.6 us (3%)
  between operations  14.3 us (1%)
  starting transfers between devices  13 us (1%)
    all_to_all x1, waiting for transfers between devices, local(): lax.all_to_all(up_cols, 'fs', split_axis=2, concat_axis=1, tiled=True)  207 us
    all_to_all x1, blocking collectives, local(): lax.all_to_all(gate_cols, 'fs', split_axis=2, concat_axis=1, tiled=True)  167 us
    reduce_scatter x1, waiting for transfers between devices, local(): lax.psum_scatter(jnp.einsum('kxh,xhd->kxd', hidden, down_weight, preferre...  89.6 us
    all_to_all x1, blocking collectives, local(): lax.all_to_all(down_half, 'tp', split_axis=0, concat_axis=2, tiled=True)  89 us
    all_to_all x1, blocking collectives, local(): lax.all_to_all(up_half, 'tp', split_axis=0, concat_axis=2, tiled=True)  86.8 us
    unnamed x26, local copies, waits for them, and re-layouts  56.9 us
    all_to_all x1, waiting for transfers between devices, local(): lax.all_to_all(gate_half, 'tp', split_axis=0, concat_axis=2, tiled=True)  50.4 us
    all_to_all x3, local copies, waits for them, and re-layouts, local(): lax.all_to_all(up_cols, 'fs', split_axis=2, concat_axis=1, tiled=True)  29 us
  transfers between devices with their start and end apart: 8, of which 4 were waited for; matrix products, arithmetic and copies ran while one was open for 15% of the time, Pallas kernels for 0%

commit v1 on v0

--- a/solution.py
+++ b/solution.py
@@ -1,15 +1,288 @@
+import functools
+
 import jax
 import jax.numpy as jnp
 from jax import lax
+from jax.experimental import pallas as pl
+from jax.experimental.pallas import tpu as pltpu
 from jax.sharding import PartitionSpec as P
 
 CAP = 32
 
 
 epsilon = 1e-06
-
-
-def local(tokens, route_ids, route_logits, norm_gain, gate_master, up_master, down_master):
+MESH = pl.DeviceIdType.MESH
+BF16 = jnp.bfloat16
+
+
+def exchange_kernel(
+    n_gr, n_fs, n_tp,
+    gain_ref, gate_ref, up_ref, down_ref,
+    gate_out, up_out, down_out,
+    stage, stage_down, crossed, raw, raw_down,
+    load_sem, load_down_sem, x_send, x_recv, s_send, s_recv, own_sem,
+    d_send, d_recv, xd_send, xd_recv, own_down_sem, dd_send, dd_recv,
+):
+    gr, fs, tp = (lax.axis_index(name) for name in ("gr", "fs", "tp"))
+    experts, _, width = gate_out.shape
+    rows, cols = gate_ref.shape[1], gate_ref.shape[2]
+    per = cols // width
+    down_cols = down_ref.shape[2]
+    masters, outs = (gate_ref, up_ref), (gate_out, up_out)
+
+    barrier = pltpu.get_barrier_semaphore()
+    peers = 0
+    for o in range(1, n_tp):
+        pl.semaphore_signal(barrier, 1, device_id=(gr, fs, lax.rem(tp + o, n_tp)), device_id_type=MESH)
+        peers += 1
+    for k in range(1, n_fs):
+        pl.semaphore_signal(barrier, 1, device_id=(gr, lax.rem(fs + k, n_fs), tp), device_id_type=MESH)
+        peers += 1
+    for o in range(1, n_gr):
+        pl.semaphore_signal(barrier, 1, device_id=(lax.rem(gr + o, n_gr), fs, tp), device_id_type=MESH)
+        peers += 1
+
+    def tp_at(o):
+        return lax.rem(tp + o, n_tp)
+
+    order = [(w, o) for w in range(2) for o in [*range(1, n_tp), 0]]
+
+    def load(e, w, o):
+        return pltpu.make_async_copy(
+            masters[w].at[tp_at(o) * experts + e], raw.at[w, o], load_sem.at[w, o]
+        )
+
+    def load_down(e, o):
+        return pltpu.make_async_copy(
+            down_ref.at[tp_at(o) * experts + e], raw_down.at[o], load_down_sem.at[o]
+        )
+
+    def over_tp(e, w, o):
+        return pltpu.make_async_remote_copy(
+            stage.at[w, o, e], crossed.at[w, o - 1, e],
+            x_send.at[w, o - 1, e], x_recv.at[w, o - 1, e],
+            device_id=(gr, fs, tp_at(o)), device_id_type=MESH,
+        )
+
+    def rows_of(group, owner):
+        return pl.ds(pl.multiple_of((group * n_fs + owner) * rows, rows), rows)
+
+    def source(e, w, o, j):
+        columns = pl.ds(j * width, width)
+        if o == 0:
+            return stage.at[w, 0, e, :, columns]
+        return crossed.at[w, o - 1, e, :, columns]
+
+    def fan(e, w, o):
+        begin = lax.rem(tp - o + n_tp, n_tp) * per
+        for j in range(per):
+            to = begin + j
+            k = lax.rem(to - fs + n_fs, n_fs)
+            target = outs[w].at[e, rows_of(gr, fs)]
+
+            @pl.when(to != fs)
+            def _():
+                pltpu.make_async_remote_copy(
+                    source(e, w, o, j), target, s_send.at[w, e, k], s_recv.at[w, e, k],
+                    device_id=(gr, to, tp), device_id_type=MESH,
+                ).start()
+
+            @pl.when(to == fs)
+            def _():
+                pltpu.make_async_copy(source(e, w, o, j), target, own_sem.at[w, e]).start()
+
+    def arrival(e, w, k):
+        piece = outs[w].at[e, rows_of(gr, lax.rem(fs - k + n_fs, n_fs))]
+        return pltpu.make_async_remote_copy(
+            piece, piece, s_send.at[w, e, k], s_recv.at[w, e, k],
+            device_id=(gr, lax.rem(fs + k, n_fs), tp), device_id_type=MESH,
+        )
+
+    def own_copy(e, w):
+        return pltpu.make_async_copy(
+            source(e, w, 0, 0), outs[w].at[e, rows_of(gr, fs)], own_sem.at[w, e]
+        )
+
+    def over_gr(e, w, k, o, group):
+        piece = outs[w].at[e, rows_of(group, lax.rem(fs - k + n_fs, n_fs))]
+        return pltpu.make_async_remote_copy(
+            piece, piece, d_send.at[w, e, k, o - 1], d_recv.at[w, e, k, o - 1],
+            device_id=(lax.rem(gr + o, n_gr), fs, tp), device_id_type=MESH,
+        )
+
+    def down_block(group, t):
+        return pl.ds(pl.multiple_of((group * n_tp + t) * down_cols, down_cols), down_cols)
+
+    def down_over_tp(e, o):
+        return pltpu.make_async_remote_copy(
+            stage_down.at[o, e], down_out.at[e, :, down_block(gr, tp)],
+            xd_send.at[o - 1, e], xd_recv.at[o - 1, e],
+            device_id=(gr, fs, tp_at(o)), device_id_type=MESH,
+        )
+
+    def down_arrival(e, o):
+        piece = down_out.at[e, :, down_block(gr, lax.rem(tp - o + n_tp, n_tp))]
+        return pltpu.make_async_remote_copy(
+            piece, piece, xd_send.at[o - 1, e], xd_recv.at[o - 1, e],
+            device_id=(gr, fs, tp_at(o)), device_id_type=MESH,
+        )
+
+    def down_own(e):
+        return pltpu.make_async_copy(
+            stage_down.at[0, e], down_out.at[e, :, down_block(gr, tp)], own_down_sem.at[e]
+        )
+
+    def down_over_gr(e, s, o, group):
+        piece = down_out.at[e, :, down_block(group, lax.rem(tp - s + n_tp, n_tp))]
+        return pltpu.make_async_remote_copy(
+            piece, piece, dd_send.at[e, s, o - 1], dd_recv.at[e, s, o - 1],
+            device_id=(lax.rem(gr + o, n_gr), fs, tp), device_id_type=MESH,
+        )
+
+    for w, o in order:
+        load(0, w, o).start()
+    for o in range(n_tp):
+        load_down(0, o).start()
+    pl.semaphore_wait(barrier, peers)
+
+    @pl.loop(0, experts)
+    def _(e):
+        for w, o in order:
+            load(e, w, o).wait()
+            stage[w, o, e] = (raw[w, o] * gain_ref[...]).astype(BF16)
+
+            @pl.when(e + 1 < experts)
+            def _():
+                load(e + 1, w, o).start()
+
+            if o:
+                over_tp(e, w, o).start()
+            else:
+                fan(e, w, 0)
+
+    @pl.loop(0, experts)
+    def _(e):
+        for o in [*range(1, n_tp), 0]:
+            load_down(e, o).wait()
+            stage_down[o, e] = raw_down[o].astype(BF16)
+
+            @pl.when(e + 1 < experts)
+            def _():
+                load_down(e + 1, o).start()
+
+            if o:
+                down_over_tp(e, o).start()
+            else:
+                down_own(e).start()
+
+    def forward(e):
+        for w in range(2):
+            for o in range(1, n_tp):
+                over_tp(e, w, o).wait_recv()
+                fan(e, w, o)
+
+    def collect(e):
+        for w in range(2):
+            own_copy(e, w).wait()
+            for o in range(1, n_gr):
+                over_gr(e, w, 0, o, gr).start()
+
+        @pl.loop(1, n_fs)
+        def _(k):
+            for w in range(2):
+                arrival(e, w, k).wait_recv()
+                for o in range(1, n_gr):
+                    over_gr(e, w, k, o, gr).start()
+
+    forward(0)
+
+    @pl.loop(1, experts)
+    def _(e):
+        forward(e)
+        collect(e - 1)
+
+    @pl.loop(0, experts)
+    def _(e):
+        down_own(e).wait()
+        for s in range(1, n_tp):
+            down_arrival(e, s).wait_recv()
+        for s in range(n_tp):
+            for o in range(1, n_gr):
+                down_over_gr(e, s, o, gr).start()
+
+    collect(experts - 1)
+
+    @pl.loop(0, experts)
+    def _(e):
+        for w in range(2):
+            for o in range(1, n_tp):
+                over_tp(e, w, o).wait_send()
+
+            @pl.loop(1, n_fs)
+            def _(k):
+                arrival(e, w, k).wait_send()
+
+            @pl.loop(0, n_fs)
+            def _(k):
+                for o in range(1, n_gr):
+                    over_gr(e, w, k, o, gr).wait_send()
+                    over_gr(e, w, k, o, lax.rem(gr - o + n_gr, n_gr)).wait_recv()
+
+        for s in range(1, n_tp):
+            down_over_tp(e, s).wait_send()
+        for s in range(n_tp):
+            for o in range(1, n_gr):
+                down_over_gr(e, s, o, gr).wait_send()
+                down_over_gr(e, s, o, lax.rem(gr - o + n_gr, n_gr)).wait_recv()
+
+
+def exchange(sizes, norm_gain, gate_master, up_master, down_master):
+    n_gr, n_fs, n_tp = sizes
+    all_experts, rows, cols = gate_master.shape
+    experts = all_experts // n_tp
+    width = cols * n_tp // n_fs
+    hidden, down_cols = down_master.shape[1], down_master.shape[2]
+    any_spec = pl.BlockSpec(memory_space=pl.ANY)
+    dma = pltpu.SemaphoreType.DMA
+    up_shape = jax.ShapeDtypeStruct((experts, rows * n_gr * n_fs, width), BF16)
+    return pl.pallas_call(
+        functools.partial(exchange_kernel, n_gr, n_fs, n_tp),
+        out_shape=(
+            up_shape,
+            up_shape,
+            jax.ShapeDtypeStruct((experts, hidden, down_cols * n_gr * n_tp), BF16),
+        ),
+        in_specs=[pl.BlockSpec(memory_space=pltpu.VMEM), any_spec, any_spec, any_spec],
+        out_specs=(any_spec, any_spec, any_spec),
+        scratch_shapes=[
+            pltpu.VMEM((2, n_tp, experts, rows, cols), BF16),
+            pltpu.VMEM((n_tp, experts, hidden, down_cols), BF16),
+            pltpu.VMEM((2, n_tp - 1, experts, rows, cols), BF16),
+            pltpu.VMEM((2, n_tp, rows, cols), jnp.float32),
+            pltpu.VMEM((n_tp, hidden, down_cols), jnp.float32),
+            dma((2, n_tp)),
+            dma((n_tp,)),
+            dma((2, n_tp - 1, experts)),
+            dma((2, n_tp - 1, experts)),
+            dma((2, experts, n_fs)),
+            dma((2, experts, n_fs)),
+            dma((2, experts)),
+            dma((2, experts, n_fs, n_gr - 1)),
+            dma((2, experts, n_fs, n_gr - 1)),
+            dma((n_tp - 1, experts)),
+            dma((n_tp - 1, experts)),
+            dma((experts,)),
+            dma((experts, n_tp, n_gr - 1)),
+            dma((experts, n_tp, n_gr - 1)),
+        ],
+        compiler_params=pltpu.CompilerParams(
+            collective_id=0, has_side_effects=True, vmem_limit_bytes=52 * 1024 * 1024
+        ),
+        cost_estimate=pl.CostEstimate(flops=0, bytes_accessed=1_000_000_000, transcendentals=0),
+    )(norm_gain[:, None], gate_master, up_master, down_master)
+
+
+def plain_local(tokens, route_ids, route_logits, norm_gain, gate_master, up_master, down_master):
     gain_rows = norm_gain[None, :, None]
     gate_half = (gate_master * gain_rows).astype(jnp.bfloat16)
     up_half = (up_master * gain_rows).astype(jnp.bfloat16)
@@ -68,7 +341,57 @@
     return (gate_weight, up_weight, down_weight, mixed)
 
 
+def fast_local(sizes, tokens, route_ids, route_logits, norm_gain, gate_master, up_master, down_master):
+    n_gr, n_fs, n_tp = sizes
+    gate_weight, up_weight, down_weight = exchange(
+        sizes, norm_gain, gate_master, up_master, down_master
+    )
+    as_float = tokens.astype(jnp.float32)
+    normed = (
+        as_float * lax.rsqrt(jnp.mean(as_float * as_float, axis=-1, keepdims=True) + epsilon)
+    ).astype(jnp.bfloat16)
+    differ = route_logits[:, 0] - route_logits[:, 1]
+    route_weight = jnp.stack([jax.nn.sigmoid(differ), jax.nn.sigmoid(-differ)], axis=1)
+    experts_here = gate_weight.shape[0]
+    first_expert = lax.axis_index("tp") * experts_here
+    expert_ids = first_expert + jnp.arange(experts_here, dtype=jnp.int32)
+    route_hits = route_ids[None, :, :] == expert_ids[:, None, None]
+    chosen = jnp.any(route_hits, axis=2)
+    weight_rows = jnp.sum(jnp.where(route_hits, route_weight[None, :, :], 0.0), axis=2)
+    slot_rank = jnp.cumsum(chosen.astype(jnp.int32), axis=1) - 1
+    slot_ids = jnp.arange(CAP, dtype=jnp.int32)
+    picker = chosen[:, None, :] & (slot_rank[:, None, :] == slot_ids[None, :, None])
+    picker_float = picker.astype(jnp.float32)
+    packed = jnp.einsum(
+        "xsr,rd->sxd", picker.astype(jnp.bfloat16), normed, preferred_element_type=jnp.float32
+    ).astype(jnp.bfloat16)
+    slot_weight = jnp.einsum(
+        "xsr,xr->sx", picker_float, weight_rows, precision=lax.Precision.HIGHEST
+    )
+    pieces = lax.all_gather(packed, "fs", axis=0, tiled=True)
+    gate_act = jnp.einsum("kxd,xdh->kxh", pieces, gate_weight, preferred_element_type=jnp.float32)
+    up_act = jnp.einsum("kxd,xdh->kxh", pieces, up_weight, preferred_element_type=jnp.float32)
+    hidden = (jax.nn.silu(gate_act) * up_act).astype(jnp.bfloat16)
+    partial = jnp.einsum(
+        "kxh,xhd->kxd", hidden, down_weight, preferred_element_type=jnp.float32
+    ).astype(jnp.bfloat16)
+    pairs, rest = n_fs // 2, (partial.shape[0] // n_fs, *partial.shape[1:])
+    partial = lax.psum_scatter(
+        partial.reshape(pairs, 2, *rest), "fs", scatter_dimension=1,
+        axis_index_groups=[[2 * i, 2 * i + 1] for i in range(pairs)],
+    )
+    expert_out = lax.psum_scatter(
+        partial, "fs", scatter_dimension=0,
+        axis_index_groups=[[2 * i + j for i in range(pairs)] for j in range(2)],
+    ).astype(jnp.float32)
+    weighted = expert_out * slot_weight[:, :, None]
+    block_sum = jnp.einsum("xsr,sxd->rd", picker_float, weighted, precision=lax.Precision.HIGHEST)
+    mixed = lax.psum(block_sum.astype(jnp.bfloat16), "tp")
+    return (gate_weight, up_weight, down_weight, mixed)
+
+
 def solution(mesh):
+    n_gr, n_fs, n_tp = (mesh.shape[name] for name in ("gr", "fs", "tp"))
     placed = (
         P(("gr", "fs"), None),
         P(("gr", "fs"), None),
@@ -78,6 +401,14 @@
         P(None, ("gr", "fs"), "tp"),
         P(None, "fs", ("gr", "tp")),
     )
+
+    def local(tokens, route_ids, route_logits, norm_gain, gate_master, up_master, down_master):
+        width = gate_master.shape[2] * n_tp // n_fs
+        aligned = width % 128 == 0 and down_master.shape[2] % 128 == 0
+        fits = n_fs % n_tp == 0 and n_fs % 2 == 0 and min(n_gr, n_tp) > 1
+        run = functools.partial(fast_local, (n_gr, n_fs, n_tp)) if aligned and fits else plain_local
+        return run(tokens, route_ids, route_logits, norm_gain, gate_master, up_master, down_master)
+
     return jax.shard_map(
         local,
         mesh=mesh,

time: 959 us -> 628 us (0.65)
  Pallas kernels: 0 us -> 367 us
  blocking collectives: 343 us -> 0 us
  waiting for transfers between devices: 358 us -> 167 us
  local copies, waits for them, and re-layouts: 165 us -> 40.5 us
  other arithmetic: 25.6 us -> 2.42 us
  starting transfers between devices: 13 us -> 0.16 us
    pallas_call x0 -> x1, Pallas kernels: none -> 367 us  [exchange(): pl.pallas_call(functools.partial(exchange_kernel, n_gr, n_fs, n_tp), out_...]
    all_to_all x3 -> x0, blocking collectives: 343 us -> none  [the longest x1 167 us: local(): lax.all_to_all(gate_cols, 'fs', split_axis=2, concat_axis=1, tiled=True)]
    all_to_all x2 -> x0, waiting for transfers between devices: 258 us -> none  [the longest x1 207 us: local(): lax.all_to_all(up_cols, 'fs', split_axis=2, concat_axis=1, tiled=True)]
    all_to_all x11 -> x0, local copies, waits for them, and re-layouts: 108 us -> none  [the longest x3 29 us: local(): lax.all_to_all(up_cols, 'fs', split_axis=2, concat_axis=1, tiled=True)]
    reduce_scatter x1 -> x2, waiting for transfers between devices: 89.6 us -> 139 us  [the longest x1 93.1 us: fast_local(): lax.psum_scatter(partial.reshape(pairs, 2, *rest), 'fs', scatter_dimensio...]
    psum x1, waiting for transfers between devices: 0.01 us -> 28 us  [fast_local(): mixed = lax.psum(block_sum.astype(jnp.bfloat16), 'tp')]
    convert_element_type x3 -> x1, other arithmetic: 24.9 us -> 0.01 us  [fast_local(): slot_rank = jnp.cumsum(chosen.astype(jnp.int32), axis=1) - 1]
    unnamed x26 -> x18, local copies, waits for them, and re-layouts: 56.9 us -> 34.9 us
  transfers between devices with their start and end apart: 8 -> 4, of which waited for: 4 -> 3; matrix products, arithmetic and copies ran while one was open for 15% -> 0% of each run, Pallas kernels for 0% -> 58%
where the time goes in v1:
time: 628 us
  Pallas kernels  367 us (58%)
  waiting for transfers between devices  167 us (27%)
  local copies, waits for them, and re-layouts  40.5 us (6%)
  matrix products  37.1 us (6%)
  between operations  13.9 us (2%)
    pallas_call x1, Pallas kernels, exchange(): pl.pallas_call(functools.partial(exchange_kernel, n_gr, n_fs, n_tp), out_...  367 us
    reduce_scatter x1, waiting for transfers between devices, fast_local(): lax.psum_scatter(partial.reshape(pairs, 2, *rest), 'fs', scatter_dimensio...  93.1 us
    reduce_scatter x1, waiting for transfers between devices, fast_local(): lax.psum_scatter(partial, 'fs', scatter_dimension=0, axis_index_groups=[[...  45.6 us
    unnamed x18, local copies, waits for them, and re-layouts  34.9 us
    psum x1, waiting for transfers between devices, fast_local(): mixed = lax.psum(block_sum.astype(jnp.bfloat16), 'tp')  28 us
    dot_general x1, matrix products, fast_local(): jnp.einsum('kxh,xhd->kxd', hidden, down_weight, preferred_element_type=jn...  21.2 us
  transfers between devices with their start and end apart: 4, of which 3 were waited for; matrix products, arithmetic and copies ran while one was open for 0% of the time, Pallas kernels for 58%

profile of v1, /device:TPU:0, one launch (start us, length us, event | category | flops | bytes accessed | tf_op | source)
XLA Modules:
  0.0 627.6 jit_solution(5159796533920175351)
XLA Ops:
  7.2 0.0 all-gather.2.cloned.1.call-start
  7.2 0.8 compare_reduce_fusion
  8.0 0.3 reduce_window_sum.11
  8.3 1.2 fusion.7
  9.5 2.2 fusion.5
  11.8 0.0 reduce-scatter.3.cloned.1.call-start
  11.8 0.8 copy.17.gain_ref
  12.6 366.8 %shard_map.102 = (bf16[4,2048,896]{2,1,0:T(8,128)(2,1)}, bf16[4,2048,896]{2,1,0:T(8,128)(2,1)}, bf16[4,896,2048]{2,1,0:T(8,128)(2,1)}) custom-call(f32[128,1]{1,0:T(8,128)S(1)} %copy.17.gain_ref, f32[8,128,3584]{2,1,0:T(8,128)} %gate_ref.1, f32[8,128,3584]{2,1,0:T(8,128)} %up_ref.1, f32[8,896,512]{2,1,0:T(8,128)} %down_ref.1), custom_call_target="tpu_custom_call" | custom-call | bytes 1000000000 | tf_op jit(solution)/shard_map/pallas_call | solution.py:248
  379.4 0.0 all-gather.2.cloned.1.call-done
  379.4 10.8 %fusion.27 = f32[4,896,256]{2,1,0:T(8,128)} fusion(bf16[4,2048,896]{2,1,0:T(8,128)(2,1)} %get-tuple-element.17, bf16[256,4,2048]{2,0,1:T(8,128)(2,1)} %all-gather.2.cloned.1.call-done), kind=kOutput, calls=%fused_computation.42 | convolution fusion | flops 3758096384 | bytes 22544384 | tf_op jit(solution)/shard_map/kxd,xdh->kxh/dot_general | solution.py:373
  390.2 21.2 %convolution_convert_fusion = bf16[4,2048,256]{1,2,0:T(8,128)(2,1)} fusion(bf16[4,896,2048]{2,1,0:T(8,128)(2,1)} %get-tuple-element.18, f32[4,896,256]{2,1,0:T(8,128)} %fusion.27, bf16[4,2048,896]{2,1,0:T(8,128)(2,1)} %get-tuple-element.16, bf16[256,4,2048]{2,0,1:T(8,128)(2,1)} %all-gather.2.cloned.1.call-done), kind=kOutput, calls=%fused_computation | convolution fusion | flops 7523794944 | bytes 41418752 | tf_op jit(solution)/shard_map/kxh,xhd->kxd/dot_general | solution.py:375
  411.5 4.8 copy.20
  416.3 0.0 reduce-scatter.5.cloned.1.call-start
  416.3 93.1 %reduce-scatter.3.cloned.1.call-done = bf16[4,1,32,4,2048]{4,2,3,0,1:T(8,128)(2,1)} async-done(((bf16[4,2,32,4,2048]{4,2,3,0,1:T(8,128)(2,1)}), bf16[4,1,32,4,2048]{4,2,3,0,1:T(8,128)(2,1)}) %reduce-scatter.3.cloned.1.call-update) | async-done | bytes 2097168 | tf_op jit(solution)/shard_map/reduce_scatter | solution.py:379
  509.5 0.0 all-reduce.2.cloned.1.call-start
  509.6 0.1 fusion.25
  509.7 0.2 fusion.16
  509.8 45.6 %reduce-scatter.5.cloned.1.call-done = bf16[1,32,4,2048]{3,1,2,0:T(8,128)(2,1)} async-done(((bf16[4,32,4,2048]{3,1,2,0:T(8,128)(2,1)}), bf16[1,32,4,2048]{3,1,2,0:T(8,128)(2,1)}) %reduce-scatter.5.cloned.1.call-update) | async-done | bytes 524304 | tf_op jit(solution)/shard_map/reduce_scatter | solution.py:383
  555.4 2.7 fusion.4
  558.1 28.0 %all-reduce.2.cloned.1.call-done = bf16[128,2048]{1,0:T(8,128)(2,1)} async-done(((bf16[128,2048]{1,0:T(8,128)(2,1)}), bf16[128,2048]{1,0:T(8,128)(2,1)}) %all-reduce.2.cloned.1.call-update) | async-done | bytes 524304 | tf_op jit(solution)/shard_map/psum | solution.py:389
  586.1 14.6 %copy.29 = bf16[4,2048,896]{2,1,0:T(8,128)(2,1)} copy(bf16[4,2048,896]{2,1,0:T(8,128)(2,1)} %get-tuple-element.16) | data formatting | bytes 29360128
  600.7 14.1 %copy.30 = bf16[4,2048,896]{2,1,0:T(8,128)(2,1)} copy(bf16[4,2048,896]{2,1,0:T(8,128)(2,1)} %get-tuple-element.17) | data formatting | bytes 29360128
  614.8 5.5 copy.31
  620.2 0.8 copy.32
  (25 shorter events, 0.1 us)
Async XLA Ops:
  7.2 372.3 %all-gather.2.cloned.1.call-start = ((), (), s32[]{:S(2)}) async-start(), calls=%async_computation.2 | async-start | bytes 4718592 | tf_op jit(solution)/shard_map/all_gather | solution.py:371
  11.8 497.7 %reduce-scatter.3.cloned.1.call-start = ((), (), s32[]{:S(2)}) async-start(), calls=%async_computation.3 | async-start | bytes 6291456 | tf_op jit(solution)/shard_map/reduce_scatter | solution.py:379
  416.3 93.3 %copy-start.2 = (f32[128,2]{0,1:T(2,128)S(1)}, f32[128,2]{0,1:T(2,128)}, u32[]{:S(2)}) copy-start(f32[128,2]{0,1:T(2,128)} %param.9) | copy-start | bytes 3076
  416.3 93.3 %copy-start.1 = (s32[128,2]{0,1:T(2,128)S(1)}, s32[128,2]{0,1:T(2,128)}, u32[]{:S(2)}) copy-start(s32[128,2]{0,1:T(2,128)} %param.8) | copy-start | bytes 3076
  416.3 139.1 %reduce-scatter.5.cloned.1.call-start = ((), (), s32[]{:S(2)}) async-start(), calls=%async_computation.4 | async-start | bytes 2621440 | tf_op jit(solution)/shard_map/reduce_scatter | solution.py:383
  509.5 76.6 %all-reduce.2.cloned.1.call-start = ((), (), s32[]{:S(2)}) async-start(), calls=%async_computation.5 | async-start | bytes 1048576 | tf_op jit(solution)/shard_map/psum | solution.py:389
  586.1 28.6 %slice-start = ((s8[14680064]{0:T(1024)(128)(4,1)}), s8[4194304]{0:T(1024)(128)(4,1)S(1)}, s32[]{:S(2)}) async-start(s8[14680064]{0:T(1024)(128)(4,1)} %bitcast.54), calls=%async_computation.6 | async-start | bytes 8388608
  586.1 28.6 %slice-start.1 = ((s8[14680064]{0:T(1024)(128)(4,1)}), s8[4194304]{0:T(1024)(128)(4,1)S(1)}, s32[]{:S(2)}) async-start(s8[14680064]{0:T(1024)(128)(4,1)} %bitcast.54), calls=%async_computation.7 | async-start | bytes 8388608
  600.7 14.1 %slice-start.2 = ((s8[14680064]{0:T(1024)(128)(4,1)}), s8[4194304]{0:T(1024)(128)(4,1)S(1)}, s32[]{:S(2)}) async-start(s8[14680064]{0:T(1024)(128)(4,1)} %bitcast.54), calls=%async_computation.8 | async-start | bytes 8388608
  600.7 14.1 %slice-start.3 = ((s8[14680064]{0:T(1024)(128)(4,1)}), s8[2097152]{0:T(1024)(128)(4,1)S(1)}, s32[]{:S(2)}) async-start(s8[14680064]{0:T(1024)(128)(4,1)} %bitcast.54), calls=%async_computation.9 | async-start | bytes 4194304
  614.8 5.5 copy-start
Sparse Core Ops, SparseCore 0:
  11.9 280.6 all-gather.1
  416.4 93.0 reduce-scatter.2
  511.8 43.5 reduce-scatter.4
  558.2 27.8 all-reduce.1

commit v2 on v1

--- a/solution.py
+++ b/solution.py
@@ -282,6 +282,178 @@
     )(norm_gain[:, None], gate_master, up_master, down_master)
 
 
+def experts_kernel(pieces, gate_in, up_in, down_in, gate_out, up_out, down_out, partial, gate_act, up_act, hidden):
+    depth = 256
+    gate_act[...] = jnp.zeros_like(gate_act)
+    up_act[...] = jnp.zeros_like(up_act)
+
+    @pl.loop(0, gate_in.shape[1] // depth)
+    def _(i):
+        span = pl.ds(pl.multiple_of(i * depth, depth), depth)
+        x = pieces[0, :, span]
+        gate = gate_in[0, span, :]
+        gate_out[0, span, :] = gate
+        gate_act[...] += jnp.dot(x, gate, preferred_element_type=jnp.float32)
+        up = up_in[0, span, :]
+        up_out[0, span, :] = up
+        up_act[...] += jnp.dot(x, up, preferred_element_type=jnp.float32)
+
+    hidden[...] = (jax.nn.silu(gate_act[...]) * up_act[...]).astype(BF16)
+
+    @pl.loop(0, down_in.shape[2] // depth)
+    def _(i):
+        span = pl.ds(pl.multiple_of(i * depth, depth), depth)
+        down = down_in[0, :, span]
+        down_out[0, :, span] = down
+        partial[0, :, span] = jnp.dot(
+            hidden[...], down, preferred_element_type=jnp.float32
+        ).astype(BF16)
+
+
+def run_experts(pieces, gate, up, down):
+    experts, features, width = gate.shape
+    count = pieces.shape[1]
+
+    def whole(*shape):
+        return pl.BlockSpec((1, *shape), lambda e: (e, 0, 0))
+
+    weights = [whole(features, width), whole(features, width), whole(width, features)]
+    return pl.pallas_call(
+        experts_kernel,
+        grid=(experts,),
+        out_shape=(
+            jax.ShapeDtypeStruct(gate.shape, BF16),
+            jax.ShapeDtypeStruct(up.shape, BF16),
+            jax.ShapeDtypeStruct(down.shape, BF16),
+            jax.ShapeDtypeStruct(pieces.shape, BF16),
+        ),
+        in_specs=[whole(count, features), *weights],
+        out_specs=(*weights, whole(count, features)),
+        scratch_shapes=[
+            pltpu.VMEM((count, width), jnp.float32),
+            pltpu.VMEM((count, width), jnp.float32),
+            pltpu.VMEM((count, width), BF16),
+        ],
+        compiler_params=pltpu.CompilerParams(vmem_limit_bytes=60 * 1024 * 1024),
+    )(pieces, gate, up, down)
+
+
+def combine_kernel(
+    n_fs, n_tp, part, combiner, out,
+    near, summed, far, total, block, others,
+    y_send, y_recv, z_send, z_recv, t_send, t_recv,
+):
+    gr, fs, tp = (lax.axis_index(name) for name in ("gr", "fs", "tp"))
+    pairs = n_fs // 2
+    z, y = fs // 2, lax.rem(fs, 2)
+    experts, _, _, cap, features = part.shape
+
+    barrier = pltpu.get_barrier_semaphore()
+    pl.semaphore_signal(barrier, 1, device_id=(gr, z * 2 + 1 - y, tp), device_id_type=MESH)
+    for k in range(1, pairs):
+        pl.semaphore_signal(
+            barrier, 1, device_id=(gr, lax.rem(z + k, pairs) * 2 + y, tp), device_id_type=MESH
+        )
+    for o in range(1, n_tp):
+        pl.semaphore_signal(barrier, 1, device_id=(gr, fs, lax.rem(tp + o, n_tp)), device_id_type=MESH)
+    pl.semaphore_wait(barrier, pairs + n_tp - 1)
+
+    def over_pair(e):
+        return pltpu.make_async_remote_copy(
+            part.at[e, :, 1 - y], near.at[e], y_send.at[e], y_recv.at[e],
+            device_id=(gr, z * 2 + 1 - y, tp), device_id_type=MESH,
+        )
+
+    def over_pairs(e, k):
+        to = lax.rem(z + k, pairs)
+        return pltpu.make_async_remote_copy(
+            summed.at[e, to], far.at[k - 1, e], z_send.at[k - 1, e], z_recv.at[k - 1, e],
+            device_id=(gr, to * 2 + y, tp), device_id_type=MESH,
+        )
+
+    def over_tp(o):
+        return pltpu.make_async_remote_copy(
+            block, others.at[o - 1], t_send.at[o - 1], t_recv.at[o - 1],
+            device_id=(gr, fs, lax.rem(tp + o, n_tp)), device_id_type=MESH,
+        )
+
+    @pl.loop(0, experts)
+    def _(e):
+        over_pair(e).start()
+
+    @pl.loop(0, experts)
+    def _(e):
+        over_pair(e).wait_recv()
+        summed[e] = (part[e, :, y].astype(jnp.float32) + near[e].astype(jnp.float32)).astype(BF16)
+        for k in range(1, pairs):
+            over_pairs(e, k).start()
+
+    @pl.loop(0, experts)
+    def _(e):
+        value = summed[e, z].astype(jnp.float32)
+        for k in range(1, pairs):
+            over_pairs(e, k).wait_recv()
+            value = value + far[k - 1, e].astype(jnp.float32)
+        total[pl.ds(pl.multiple_of(e * cap, cap), cap), :] = value
+
+    tile = 512
+
+    @pl.loop(0, features // tile)
+    def _(i):
+        span = pl.ds(pl.multiple_of(i * tile, tile), tile)
+        block[:, span] = jnp.dot(
+            combiner[...], total[:, span], preferred_element_type=jnp.float32,
+            precision=lax.Precision.HIGHEST,
+        ).astype(BF16)
+
+    for o in range(1, n_tp):
+        over_tp(o).start()
+    mixed = block[...].astype(jnp.float32)
+    for o in range(1, n_tp):
+        over_tp(o).wait_recv()
+        mixed = mixed + others[o - 1].astype(jnp.float32)
+    out[...] = mixed.astype(BF16)
+
+    @pl.loop(0, experts)
+    def _(e):
+        over_pair(e).wait_send()
+        for k in range(1, pairs):
+            over_pairs(e, k).wait_send()
+
+    for o in range(1, n_tp):
+        over_tp(o).wait_send()
+
+
+def combine(n_fs, n_tp, partial, combiner):
+    experts, count, features = partial.shape
+    pairs, cap, tokens = n_fs // 2, count // n_fs, combiner.shape[0]
+    dma = pltpu.SemaphoreType.DMA
+    vmem = pl.BlockSpec(memory_space=pltpu.VMEM)
+    return pl.pallas_call(
+        functools.partial(combine_kernel, n_fs, n_tp),
+        out_shape=jax.ShapeDtypeStruct((tokens, features), BF16),
+        in_specs=[vmem, vmem],
+        out_specs=vmem,
+        scratch_shapes=[
+            pltpu.VMEM((experts, pairs, cap, features), BF16),
+            pltpu.VMEM((experts, pairs, cap, features), BF16),
+            pltpu.VMEM((pairs - 1, experts, cap, features), BF16),
+            pltpu.VMEM((experts * cap, features), jnp.float32),
+            pltpu.VMEM((tokens, features), BF16),
+            pltpu.VMEM((n_tp - 1, tokens, features), BF16),
+            dma((experts,)),
+            dma((experts,)),
+            dma((pairs - 1, experts)),
+            dma((pairs - 1, experts)),
+            dma((n_tp - 1,)),
+            dma((n_tp - 1,)),
+        ],
+        compiler_params=pltpu.CompilerParams(
+            collective_id=1, has_side_effects=True, vmem_limit_bytes=40 * 1024 * 1024
+        ),
+    )(partial.reshape(experts, pairs, 2, cap, features), combiner)
+
+
 def plain_local(tokens, route_ids, route_logits, norm_gain, gate_master, up_master, down_master):
     gain_rows = norm_gain[None, :, None]
     gate_half = (gate_master * gain_rows).astype(jnp.bfloat16)
@@ -343,7 +515,7 @@
 
 def fast_local(sizes, tokens, route_ids, route_logits, norm_gain, gate_master, up_master, down_master):
     n_gr, n_fs, n_tp = sizes
-    gate_weight, up_weight, down_weight = exchange(
+    gate_moved, up_moved, down_moved = exchange(
         sizes, norm_gain, gate_master, up_master, down_master
     )
     as_float = tokens.astype(jnp.float32)
@@ -352,7 +524,7 @@
     ).astype(jnp.bfloat16)
     differ = route_logits[:, 0] - route_logits[:, 1]
     route_weight = jnp.stack([jax.nn.sigmoid(differ), jax.nn.sigmoid(-differ)], axis=1)
-    experts_here = gate_weight.shape[0]
+    experts_here = gate_moved.shape[0]
     first_expert = lax.axis_index("tp") * experts_here
     expert_ids = first_expert + jnp.arange(experts_here, dtype=jnp.int32)
     route_hits = route_ids[None, :, :] == expert_ids[:, None, None]
@@ -363,30 +535,14 @@
     picker = chosen[:, None, :] & (slot_rank[:, None, :] == slot_ids[None, :, None])
     picker_float = picker.astype(jnp.float32)
     packed = jnp.einsum(
-        "xsr,rd->sxd", picker.astype(jnp.bfloat16), normed, preferred_element_type=jnp.float32
+        "xsr,rd->xsd", picker.astype(jnp.bfloat16), normed, preferred_element_type=jnp.float32
     ).astype(jnp.bfloat16)
-    slot_weight = jnp.einsum(
-        "xsr,xr->sx", picker_float, weight_rows, precision=lax.Precision.HIGHEST
-    )
-    pieces = lax.all_gather(packed, "fs", axis=0, tiled=True)
-    gate_act = jnp.einsum("kxd,xdh->kxh", pieces, gate_weight, preferred_element_type=jnp.float32)
-    up_act = jnp.einsum("kxd,xdh->kxh", pieces, up_weight, preferred_element_type=jnp.float32)
-    hidden = (jax.nn.silu(gate_act) * up_act).astype(jnp.bfloat16)
-    partial = jnp.einsum(
-        "kxh,xhd->kxd", hidden, down_weight, preferred_element_type=jnp.float32
-    ).astype(jnp.bfloat16)
-    pairs, rest = n_fs // 2, (partial.shape[0] // n_fs, *partial.shape[1:])
-    partial = lax.psum_scatter(
-        partial.reshape(pairs, 2, *rest), "fs", scatter_dimension=1,
-        axis_index_groups=[[2 * i, 2 * i + 1] for i in range(pairs)],
-    )
-    expert_out = lax.psum_scatter(
-        partial, "fs", scatter_dimension=0,
-        axis_index_groups=[[2 * i + j for i in range(pairs)] for j in range(2)],
-    ).astype(jnp.float32)
-    weighted = expert_out * slot_weight[:, :, None]
-    block_sum = jnp.einsum("xsr,sxd->rd", picker_float, weighted, precision=lax.Precision.HIGHEST)
-    mixed = lax.psum(block_sum.astype(jnp.bfloat16), "tp")
+    combiner = jnp.transpose(picker_float * weight_rows[:, None, :], (2, 0, 1))
+    pieces = lax.all_gather(packed, "fs", axis=1, tiled=True)
+    gate_weight, up_weight, down_weight, partial = run_experts(
+        pieces, gate_moved, up_moved, down_moved
+    )
+    mixed = combine(n_fs, n_tp, partial, combiner.reshape(combiner.shape[0], -1))
     return (gate_weight, up_weight, down_weight, mixed)
 
 

time: 628 us -> 545 us (0.87)
  waiting for transfers between devices: 167 us -> 0.04 us
  Pallas kernels: 367 us -> 519 us
  local copies, waits for them, and re-layouts: 40.5 us -> 4.15 us
  matrix products: 37.1 us -> 2.22 us
    pallas_call x0 -> x2, Pallas kernels: none -> 153 us  [the longest x1 112 us: combine(): pl.pallas_call(functools.partial(combine_kernel, n_fs, n_tp), out_shape=j...]
    reduce_scatter x2 -> x0, waiting for transfers between devices: 139 us -> none  [the longest x1 93.1 us: fast_local(): lax.psum_scatter(partial.reshape(pairs, 2, *rest), 'fs', scatter_dimensio...]
    dot_general x5 -> x1, matrix products: 37.1 us -> 2.22 us  [fast_local(): jnp.einsum('xsr,rd->xsd', picker.astype(jnp.bfloat16), normed, preferred_...]
    unnamed x18 -> x3, local copies, waits for them, and re-layouts: 34.9 us -> 2.98 us
    psum x1 -> x0, waiting for transfers between devices: 28 us -> none  [fast_local(): mixed = lax.psum(block_sum.astype(jnp.bfloat16), 'tp')]
  transfers between devices with their start and end apart: 4 -> 1, of which waited for: 3 -> 0; matrix products, arithmetic and copies ran while one was open for 0% -> 1% of each run, Pallas kernels for 58% -> 67%
where the time goes in v2:
time: 545 us; the launch traced here: 544 us
  Pallas kernels  519 us (95%)
  between operations  14.1 us (3%)
    pallas_call x1, Pallas kernels, exchange(): pl.pallas_call(functools.partial(exchange_kernel, n_gr, n_fs, n_tp), out_...  367 us
    pallas_call x1, Pallas kernels, combine(): pl.pallas_call(functools.partial(combine_kernel, n_fs, n_tp), out_shape=j...  112 us
    pallas_call x1, Pallas kernels, run_experts(): pl.pallas_call(experts_kernel, grid=(experts,), out_shape=(jax.ShapeDtype...  40.5 us
  transfers between devices with their start and end apart: 1, of which 0 were waited for; matrix products, arithmetic and copies ran while one was open for 1% of the time, Pallas kernels for 67%

profile of v2, /device:TPU:0, one launch (start us, length us, event | category | flops | bytes accessed | tf_op | source)
XLA Modules:
  0.0 543.8 jit_solution(8805089935193190729)
XLA Ops:
  7.2 0.0 all-gather.2.cloned.1.call-start
  7.2 0.8 compare_reduce_fusion
  8.0 0.3 reduce_window_sum.11
  8.3 1.2 fusion
  9.5 2.2 convolution_convert_fusion
  11.8 0.0 all-gather.2.cloned.1.call-update
  11.8 0.8 copy.22.gain_ref
  12.6 0.1 copy.23
  12.7 0.8 add_divide_fusion.1
  13.4 0.8 fusion.9
  14.2 0.1 copy.25
  14.3 0.1 copy.24
  14.5 0.1 eq.49
  14.5 366.7 %shard_map.102 = (bf16[4,2048,896]{2,1,0:T(8,128)(2,1)}, bf16[4,2048,896]{2,1,0:T(8,128)(2,1)}, bf16[4,896,2048]{2,1,0:T(8,128)(2,1)}) custom-call(f32[128,1]{1,0:T(8,128)S(1)} %copy.22.gain_ref, f32[8,128,3584]{2,1,0:T(8,128)} %gate_ref.1, f32[8,128,3584]{2,1,0:T(8,128)} %up_ref.1, f32[8,896,512]{2,1,0:T(8,128)} %down_ref.1), custom_call_target="tpu_custom_call" | custom-call | bytes 1000000000 | tf_op jit(solution)/shard_map/pallas_call | solution.py:248
  381.3 0.0 all-gather.2.cloned.1.call-done.pieces
  381.3 40.5 %shard_map.103 = (bf16[4,2048,896]{2,1,0:T(8,128)(2,1)}, bf16[4,2048,896]{2,1,0:T(8,128)(2,1)}, bf16[4,896,2048]{2,1,0:T(8,128)(2,1)}, bf16[4,256,2048]{2,1,0:T(8,128)(2,1)}) custom-call(bf16[4,256,2048]{2,1,0:T(8,128)(2,1)} %all-gather.2.cloned.1.call-done.pieces, bf16[4,2048,896]{2,1,0:T(8,128)(2,1)} %get-tuple-element.11.gate_in, ...), custom_call_target="tpu_custom_call" | custom-call | tf_op jit(solution)/shard_map/pallas_call | solution.py:321
  421.8 0.0 copy-start
  421.8 2.2 copy-done
  424.0 112.1 %shard_map.104 = bf16[128,2048]{1,0:T(8,128)(2,1)S(1)} custom-call(bf16[4,4,2,32,2048]{4,3,2,1,0:T(8,128)(2,1)S(1)} %bitcast.12, f32[128,128]{1,0:T(8,128)S(1)} %and_select_fusion.combiner), custom_call_target="tpu_custom_call" | custom-call | tf_op jit(solution)/shard_map/pallas_call | solution.py:432
  536.1 0.8 copy.27
  (10 shorter events, 0.1 us)
Async XLA Ops:
  7.2 374.2 %all-gather.2.cloned.1.call-start = ((), (), s32[]{:S(2)}) async-start(), calls=%async_computation | async-start | bytes 4718592 | tf_op jit(solution)/shard_map/all_gather | solution.py:541
  421.8 2.2 copy-start
Sparse Core Ops, SparseCore 0:
  11.9 275.7 all-gather.1
